TPU v7x, 32 devices: a whole 2x2x4 slice. The times are simulated.
32 devices in a mesh: ep: 8 (over z, core), tp: 4 (over y, x).
Axes of the slice: x: 2, y: 2, z: 4, core: 2. Of those that a mesh axis runs over, the one named last changes fastest.
Arguments:
- query_maps: bfloat16 [1024, 16, 128], P('ep', 'tp'), may hold values from -6 to 6
- key_maps: bfloat16 [1024, 16, 128], P('ep', 'tp'), may hold values from -6 to 6
- value_rows: bfloat16 [1024, 16, 128], P('ep', 'tp'), may hold values from -6 to 6
- head_lambda: float32 [16], P('tp'), may hold values from 0.3 to 0.8
- head_gain: float32 [128], replicated, may hold values from 0.1 to 1.9
- out_weight: bfloat16 [2048, 2048], P('tp'), may hold values from -0.125 to 0.125
- token_rows: bfloat16 [1024, 2048], P('ep'), may hold values from -36 to 36
- norm_gain: float32 [2048], replicated, may hold values from 0.1 to 1.9
- expert_ids: int32 [1024, 4], P('ep'), may hold values from 0 to 7, all different within a row; in each aligned block of 128 rows (0 to 127, 128 to 255, ...) at most 80 rows name the same one
- route_weights: float32 [1024, 4], P('ep'), may hold values from 0.1 to 0.5
- gate_weight: bfloat16 [8, 2048, 4096], P('ep', None, 'tp'), may hold values from -0.82864076 to 0.82864076
- up_weight: bfloat16 [8, 2048, 4096], P('ep', None, 'tp'), may hold values from -0.82864076 to 0.82864076
- down_weight: bfloat16 [8, 4096, 2048], P('ep', 'tp'), may hold values from -0.03125 to 0.03125
Outputs:
- mixed_rows: bfloat16 [1024, 2048], P(('ep', 'tp'))
- mixed_experts: bfloat16 [1024, 2048], P('ep', 'tp')
Inputs may be any that keep to these rules, and one draw needn't show every extreme that they name: `expert_ids`: each row names 4 different experts. Among the rows of one index of ep no expert is named more than 80 times, and in every draw some expert is named exactly 80 times there.
All inputs are finite; a program needn't handle non-finite values.
Results may differ from a plain program's by a relative error of at most 0.015.
Values may be sent and summed in bfloat16 or wider, within the bound.
A program may use at most 64 MiB of HBM per device.

v0:
```python
import functools

import jax
import jax.numpy as jnp
from jax import lax
from jax.experimental import pallas as pl
from jax.experimental.pallas import tpu as pltpu
from jax.sharding import PartitionSpec as P

NORM_EPS = 1e-05
CLAMP_LIMIT = 7.0
GATE_SLOPE = 1.702
CORES = 2
F32 = jnp.float32
BF16 = jnp.bfloat16


def remote(src, dst, send_sem, recv_sem, ep, tp):
    return pltpu.make_async_remote_copy(
        src_ref=src,
        dst_ref=dst,
        send_sem=send_sem,
        recv_sem=recv_sem,
        device_id={"ep": ep, "tp": tp},
        device_id_type=pl.DeviceIdType.MESH,
    )


def kernel(
    n_ep,
    n_tp,
    route_count,
    head_width,
    q_ref,
    k_ref,
    v_ref,
    lam_ref,
    gain_ref,
    rows_ref,
    norm_gain_ref,
    ids_ref,
    route_ref,
    ow_hbm,
    wg_hbm,
    wu_hbm,
    wd_hbm,
    out_rows_ref,
    out_exp_ref,
    ow,
    wg,
    wu,
    wd,
    xfull,
    xb,
    meta,
    kvb,
    act,
    cbuf,
    pbuf,
    rbuf,
    ubuf,
    vbuf,
    head_rows,
    prod,
    abuf,
    xs_s,
    xs_r,
    ms_s,
    ms_r,
    ks_s,
    ks_r,
    t_s,
    t_r,
    h_s,
    h_r,
    d_s,
    d_r,
    md_s,
    md_r,
    kd_s,
    kd_r,
    p_s,
    p_r,
    r_s,
    r_r,
    v_s,
    v_r,
    a_s,
    a_r,
    w_sem,
):
    nz = n_ep // CORES
    ep = lax.axis_index("ep")
    tp = lax.axis_index("tp")
    z = ep // CORES
    core = ep % CORES
    partner = z * CORES + (1 - core)
    tokens, model = rows_ref.shape
    quarter = model // n_tp
    hidden = wg.shape[1]

    weight_copies = [
        pltpu.make_async_copy(src, dst, w_sem.at[i])
        for i, (src, dst) in enumerate([(wg_hbm, wg), (wu_hbm, wu), (wd_hbm, wd), (ow_hbm, ow)])
    ]
    for copy in weight_copies:
        copy.start()

    barrier = pltpu.get_barrier_semaphore()

    def greet(e, t):
        pl.semaphore_signal(
            barrier, inc=1, device_id={"ep": e, "tp": t}, device_id_type=pl.DeviceIdType.MESH
        )

    greet(partner, tp)
    for off in range(1, nz):
        greet(((z + off) % nz) * CORES + core, tp)
    for off in range(1, n_tp):
        greet(ep, (tp + off) % n_tp)

    rows = rows_ref[...].astype(F32)
    mean_sq = jnp.mean(rows * rows, axis=-1, keepdims=True)
    xfull[...] = (rows * lax.rsqrt(mean_sq + NORM_EPS) * norm_gain_ref[...]).astype(BF16)
    xb[tp, ep] = xfull[:, pl.ds(pl.multiple_of(tp * quarter, quarter), quarter)]
    meta[ep, :route_count] = ids_ref[...].astype(F32)
    meta[ep, route_count : 2 * route_count] = route_ref[...]
    span_all = k_ref.shape[1]
    kvb[ep, :, :span_all] = k_ref[...]
    kvb[ep, :, span_all:] = v_ref[...]

    pl.semaphore_wait(barrier, 1 + (nz - 1) + (n_tp - 1))

    near = jnp.minimum(z, nz - 1 - z)
    far_sign = jnp.where(z < nz - 1 - z, 1, -1)

    def origin(i):
        alternate = ((i + 1) // 2) * ((i % 2) * 2 - 1)
        return z + jnp.where(i <= 2 * near, alternate, far_sign * (i - near))

    def line_copy(buf, send, recv, zo, way):
        block = buf.at[zo * CORES + core]
        return remote(
            block,
            block,
            send.at[way, zo],
            recv.at[zo],
            (z + (1 if way == 0 else -1)) * CORES + core,
            tp,
        )

    x_own = xb.at[tp]

    def each_line(buf, send, recv, zo, act_on):
        @pl.when((zo <= z) & (z < nz - 1))
        def _():
            act_on(line_copy(buf, send, recv, zo, 0))

        @pl.when((zo >= z) & (z > 0))
        def _():
            act_on(line_copy(buf, send, recv, zo, 1))

    square = n_tp == 4
    half = tokens // 2
    side = tp + 1 - 2 * (tp % 2)
    other = (tp + 2) % n_tp
    across = (side + 2) % n_tp
    halves = (pl.ds(0, half), pl.ds(half, half))
    targets = [side, other] if square else [(tp + off) % n_tp for off in range(1, n_tp)]

    def tp_copy(zo, n):
        block = xb.at[tp, zo * CORES + core]
        return remote(block, block, t_s.at[n, zo], t_r.at[tp, zo], ep, targets[n])

    def tp_arrival(zo, n):
        j = targets[n]
        block = xb.at[j, zo * CORES + core]
        return remote(block, block, t_s.at[n, zo], t_r.at[j, zo], ep, j)

    def pass_copy(zo, n):
        block = xb.at[other if n == 0 else side, zo * CORES + core, halves[n]]
        return remote(block, block, h_s.at[n, zo], h_r.at[n, zo], ep, targets[n])

    def pass_arrival(zo, n):
        block = xb.at[across, zo * CORES + core, halves[n]]
        return remote(block, block, h_s.at[n, zo], h_r.at[n, zo], ep, targets[n])

    def take_tp(zo):
        for n, j in enumerate(targets):
            tp_arrival(zo, n).wait_recv()
        if square:
            for n in range(2):
                pass_copy(zo, n).start()
        for n, j in enumerate(targets):
            pair_copy(j, zo).start()

    def pair_copy(j, zo, mine=True):
        block = xb.at[j, zo * CORES + (core if mine else 1 - core)]
        return remote(block, block, d_s.at[j, zo], d_r.at[j, zo], partner, tp)

    def pair_block(buf, send, recv, zo, mine=True):
        block = buf.at[zo * CORES + (core if mine else 1 - core)]
        return remote(block, block, send.at[zo], recv.at[zo], partner, tp)

    start = lambda copy: copy.start()

    def spread_x(zo):
        each_line(x_own, xs_s, xs_r, zo, start)
        for n in range(len(targets)):
            tp_copy(zo, n).start()
        pair_copy(tp, zo).start()
        each_line(meta, ms_s, ms_r, zo, start)
        pair_block(meta, md_s, md_r, zo).start()

    def spread_kv(zo):
        each_line(kvb, ks_s, ks_r, zo, start)
        pair_block(kvb, kd_s, kd_r, zo).start()

    def take_x(zo):
        line_copy(x_own, xs_s, xs_r, zo, 0).wait_recv()
        line_copy(meta, ms_s, ms_r, zo, 0).wait_recv()
        spread_x(zo)

    def take_kv(zo):
        line_copy(kvb, ks_s, ks_r, zo, 0).wait_recv()
        spread_kv(zo)

    def half_copy(zo):
        return remote(
            cbuf.at[zo, 1 - core], pbuf.at[zo], p_s.at[zo], p_r.at[zo], partner, tp
        )

    def term_parts():
        everything = pl.ds(0, tokens)
        if square:
            return [
                (side, halves[0], side, side),
                (across, halves[0], side, across),
                (other, halves[1], other, other),
                (across, halves[1], other, across),
                (other, halves[0], other, side),
                (side, halves[1], side, other),
            ]
        return [(j, everything, j, tp) for j in targets]

    def term_copy(zo, n):
        j, rows_of, device, slot = term_parts()[n]
        return remote(
            cbuf.at[zo, core, j, rows_of],
            rbuf.at[zo, slot, rows_of],
            r_s.at[n, zo],
            r_r.at[n, zo] if square else r_r.at[tp, zo],
            ep,
            device,
        )

    def term_arrival(zo, n):
        if square:
            slot = [tp, other, tp, side, across, across][n]
            rows_of = term_parts()[n][1]
            device = term_parts()[n][2]
            sem = r_r.at[n, zo]
        else:
            slot = device = targets[n]
            rows_of = pl.ds(0, tokens)
            sem = r_r.at[slot, zo]
        return remote(
            cbuf.at[zo, core, device, rows_of],
            rbuf.at[zo, slot, rows_of],
            r_s.at[n, zo],
            sem,
            ep,
            device,
        )

    def middle(zo):
        if square:
            for n in range(4):
                term_arrival(zo, n).wait_recv()
            for n, j in ((4, other), (5, side)):
                rows_of = halves[n - 4]
                cbuf[zo, core, j, rows_of] = (
                    cbuf[zo, core, j, rows_of].astype(F32) + rbuf[zo, j, rows_of].astype(F32)
                ).astype(BF16)
                term_copy(zo, n).start()

    def home_copy(zo):
        return remote(
            ubuf.at[zo], vbuf.at[z], v_s.at[zo], v_r.at[z], zo * CORES + core, tp
        )

    def home_arrival(zo):
        return remote(
            ubuf.at[zo], vbuf.at[zo], v_s.at[zo], v_r.at[zo], zo * CORES + core, tp
        )

    def finish(zo):
        half_copy(zo).wait_recv()
        for j in range(n_tp):
            cbuf[zo, core, j] = (
                cbuf[zo, core, j].astype(F32) + pbuf[zo, j].astype(F32)
            ).astype(BF16)
        for n in range(4 if square else len(targets)):
            term_copy(zo, n).start()

    def reduce(zo):
        total = cbuf[zo, core, tp].astype(F32)
        if square:
            for n in (4, 5):
                term_arrival(zo, n).wait_recv()
            total = total + rbuf[zo, tp].astype(F32) + rbuf[zo, across].astype(F32)
        else:
            for n, j in enumerate(targets):
                term_arrival(zo, n).wait_recv()
                total = total + rbuf[zo, j].astype(F32)
        ubuf[zo] = total.astype(BF16)

        @pl.when(zo != z)
        def _():
            home_copy(zo).start()

    tile = min(256, hidden)

    def experts(i, zo):
        pair = pl.ds(zo * CORES, CORES)

        def hidden_tile(f, carry):
            cols = pl.ds(pl.multiple_of(f * tile, tile), tile)
            gate = jnp.zeros((CORES * tokens, tile), F32)
            up = jnp.zeros((CORES * tokens, tile), F32)
            for j in range(n_tp):
                chunk = xb[j, pair].reshape(CORES * tokens, quarter)
                depth = pl.ds(j * quarter, quarter)
                gate = gate + jnp.dot(chunk, wg[depth, cols], preferred_element_type=F32)
                up = up + jnp.dot(chunk, wu[depth, cols], preferred_element_type=F32)
            gated = jnp.minimum(gate, CLAMP_LIMIT)
            clipped = jnp.clip(up, -CLAMP_LIMIT, CLAMP_LIMIT)
            act[:, cols] = (
                (clipped + 1.0) * gated * jax.nn.sigmoid(GATE_SLOPE * gated)
            ).astype(BF16)
            return carry

        lax.fori_loop(0, hidden // tile, hidden_tile, 0)

        @pl.when(i > 1)
        def _():
            middle(origin(i - 2))

        @pl.when(i + 1 < nz)
        def _():
            take_tp(origin(i + 1))

        @pl.when(i > 0)
        def _():
            finish(origin(i - 1))

        eye = lax.broadcasted_iota(jnp.int32, (tokens, tokens), 0) == lax.broadcasted_iota(
            jnp.int32, (tokens, tokens), 1
        )
        columns = []
        for c in range(CORES):
            info = meta[zo * CORES + c]
            named = info[:route_count] == ep.astype(F32)
            weights = jnp.where(named, info[route_count : 2 * route_count], 0.0)
            line = jnp.sum(weights, axis=0, keepdims=True)
            columns.append(jnp.sum(jnp.where(eye, line, 0.0), axis=1, keepdims=True))
        scale = jnp.concatenate(columns, axis=0)

        def model_tile(j, carry):
            cols = pl.ds(pl.multiple_of(j * quarter, quarter), quarter)
            value = jnp.dot(act[...], wd[:, cols], preferred_element_type=F32) * scale
            value = value.astype(BF16)
            for c in range(CORES):
                cbuf[zo, c, j] = value[c * tokens : (c + 1) * tokens]
            return carry

        lax.fori_loop(0, n_tp, model_tile, 0)
        half_copy(zo).start()

    spread_x(z)
    take_tp(z)

    def step(i, carry):
        zo = origin(i)

        @pl.when(i + 1 < nz)
        def _():
            take_x(origin(i + 1))

        @pl.when(i == 0)
        def _():
            spread_kv(z)

        @pl.when(i > 0)
        def _():
            take_kv(zo)

        if square:
            for n in range(2):
                pass_arrival(zo, n).wait_recv()
            pair_copy(across, zo).start()
        for j in range(n_tp):
            pair_copy(j, zo, False).wait_recv()
        pair_block(meta, md_s, md_r, zo, False).wait_recv()

        @pl.when(i == 0)
        def _():
            for copy in weight_copies[:3]:
                copy.wait()

        experts(i, zo)

        @pl.when(i > 1)
        def _():
            reduce(origin(i - 2))

        return carry

    lax.fori_loop(0, nz, step, 0)

    def wait_kv(i, carry):
        pair_block(kvb, kd_s, kd_r, i, False).wait_recv()
        return carry

    lax.fori_loop(0, nz, wait_kv, 0)
    middle(origin(nz - 2))
    finish(origin(nz - 1))

    width = 2 * head_width
    all_heads = q_ref.shape[1]
    heads = all_heads // width
    key_blocks = min(n_ep, 8)
    key_span = key_blocks * tokens
    lane = lax.broadcasted_iota(jnp.int32, (tokens, width), 1)
    gain = gain_ref[...]

    def one_head(h, carry):
        cols = pl.ds(pl.multiple_of(h * width, width), width)
        value_cols = pl.ds(pl.multiple_of(all_heads + h * width, width), width)
        query = q_ref[:, cols]
        nothing = jnp.zeros_like(query)
        both = jnp.concatenate(
            [jnp.where(lane < head_width, query, nothing), jnp.where(lane < head_width, nothing, query)],
            axis=0,
        )
        row = lax.broadcasted_iota(jnp.int32, (2 * tokens, key_span), 0) % tokens + ep * tokens
        col = lax.broadcasted_iota(jnp.int32, (2 * tokens, key_span), 1)

        def span(s, state):
            top, total, value_sum = state
            blocks = pl.ds(s * key_blocks, key_blocks)
            keys = kvb[blocks, :, cols].reshape(key_span, width)
            values = kvb[blocks, :, value_cols].reshape(key_span, width)
            score = lax.dot_general(
                both, keys, (((1,), (1,)), ((), ())), preferred_element_type=F32
            ) * (head_width**-0.5)
            score = jnp.where(col + s * key_span <= row, score, -1e30)
            new_top = jnp.maximum(top, jnp.max(score, axis=1, keepdims=True))
            terms = jnp.exp(score - new_top)
            keep = jnp.exp(top - new_top)
            total = total * keep + jnp.sum(terms, axis=1, keepdims=True)
            value_sum = value_sum * keep + jnp.dot(
                terms.astype(BF16), values, preferred_element_type=F32
            )
            return new_top, total, value_sum

        state = (
            jnp.full((2 * tokens, 1), -1e30, F32),
            jnp.zeros((2 * tokens, 1), F32),
            jnp.zeros((2 * tokens, width), F32),
        )
        if n_ep == key_blocks:
            state = span(0, state)
        else:
            state = lax.fori_loop(0, n_ep // key_blocks, span, state)
        mean = state[2] / state[1]
        attended = mean[:tokens] - lam_ref[h] * mean[tokens:]
        mean_sq = jnp.mean(attended * attended, axis=-1, keepdims=True)
        head_rows[:, cols] = (attended * lax.rsqrt(mean_sq + NORM_EPS) * gain).astype(BF16)
        return carry

    lax.fori_loop(0, heads // 2, one_head, 0)
    middle(origin(nz - 1))
    reduce(origin(nz - 2))
    lax.fori_loop(heads // 2, heads, one_head, 0)
    weight_copies[3].wait()
    out_rows = tokens // n_tp

    def product_tile(n, carry):
        cols = pl.ds(pl.multiple_of(n * quarter, quarter), quarter)
        value = jnp.dot(head_rows[...], ow[:, cols], preferred_element_type=F32).astype(BF16)
        for j in range(n_tp):
            prod[j, :, cols] = value[j * out_rows : (j + 1) * out_rows]
        return carry

    lax.fori_loop(0, n_tp, product_tile, 0)

    def row_copy(off):
        j = (tp + off) % n_tp
        return remote(prod.at[j], abuf.at[tp], a_s.at[off], a_r.at[tp], ep, j)

    def row_arrival(off):
        j = (tp + off) % n_tp
        return remote(prod.at[j], abuf.at[j], a_s.at[off], a_r.at[j], ep, j)

    for off in range(1, n_tp):
        row_copy(off).start()
    reduce(origin(nz - 1))

    mixed = prod[tp].astype(F32)
    for off in range(1, n_tp):
        row_arrival(off).wait_recv()
        mixed = mixed + abuf[(tp + off) % n_tp].astype(F32)
    out_rows_ref[...] = mixed

    combined = ubuf[z].astype(F32)
    for off in range(1, nz):
        zs = (z + off) % nz
        home_arrival(zs).wait_recv()
        combined = combined + vbuf[zs].astype(F32)
    out_exp_ref[...] = combined

    left = lambda copy: copy.wait_send()

    def drain(zo, carry):
        each_line(x_own, xs_s, xs_r, zo, left)
        each_line(meta, ms_s, ms_r, zo, left)
        each_line(kvb, ks_s, ks_r, zo, left)
        for n in range(len(targets)):
            tp_copy(zo, n).wait_send()
        for n in range(len(term_parts())):
            term_copy(zo, n).wait_send()
        if square:
            for n in range(2):
                pass_copy(zo, n).wait_send()
        for j in range(n_tp):
            pair_copy(j, zo).wait_send()
        pair_block(meta, md_s, md_r, zo).wait_send()
        pair_block(kvb, kd_s, kd_r, zo).wait_send()
        half_copy(zo).wait_send()

        @pl.when(zo != z)
        def _():
            home_copy(zo).wait_send()

        return carry

    lax.fori_loop(0, nz, drain, 0)
    for off in range(1, n_tp):
        row_copy(off).wait_send()


def body(
    query_maps,
    key_maps,
    value_rows,
    head_lambda,
    head_gain,
    out_weight,
    token_rows,
    norm_gain,
    expert_ids,
    route_weights,
    gate_weight,
    up_weight,
    down_weight,
):
    n_ep, n_tp = lax.axis_size("ep"), lax.axis_size("tp")
    nz = n_ep // CORES
    tokens, heads, width = query_maps.shape
    model = token_rows.shape[1]
    quarter = model // n_tp
    hidden = gate_weight.shape[2]
    routes = expert_ids.shape[1]
    span = heads * width
    queries = query_maps.reshape(tokens, span)
    keys = key_maps.reshape(tokens, span)
    values = value_rows.reshape(tokens, span)
    vmem = pl.BlockSpec(memory_space=pltpu.VMEM)
    smem = pl.BlockSpec(memory_space=pltpu.SMEM)
    hbm = pl.BlockSpec(memory_space=pltpu.HBM)
    dma = pltpu.SemaphoreType.DMA
    line = [dma((2, nz)), dma((nz,))]
    line_sem = [dma((2, nz)), dma((2, nz))]
    grid_sem = [dma((n_tp, nz)), dma((n_tp, nz))]
    pair = [dma((nz,)), dma((nz,))]
    mixed_rows, mixed_experts = pl.pallas_call(
        functools.partial(kernel, n_ep, n_tp, routes, width // 2),
        out_shape=(
            jax.ShapeDtypeStruct((tokens // n_tp, model), F32),
            jax.ShapeDtypeStruct((tokens, quarter), F32),
        ),
        in_specs=[vmem, vmem, vmem, smem, vmem, vmem, vmem, vmem, vmem, hbm, hbm, hbm, hbm],
        out_specs=(vmem, vmem),
        scratch_shapes=[
            pltpu.VMEM(out_weight.shape, BF16),
            pltpu.VMEM((model, hidden), BF16),
            pltpu.VMEM((model, hidden), BF16),
            pltpu.VMEM((hidden, model), BF16),
            pltpu.VMEM((tokens, model), BF16),
            pltpu.VMEM((n_tp, n_ep, tokens, quarter), BF16),
            pltpu.VMEM((n_ep, 2 * routes, tokens), F32),
            pltpu.VMEM((n_ep, tokens, 2 * span), BF16),
            pltpu.VMEM((CORES * tokens, hidden), BF16),
            pltpu.VMEM((nz, CORES, n_tp, tokens, quarter), BF16),
            pltpu.VMEM((nz, n_tp, tokens, quarter), BF16),
            pltpu.VMEM((nz, n_tp, tokens, quarter), BF16),
            pltpu.VMEM((nz, tokens, quarter), BF16),
            pltpu.VMEM((nz, tokens, quarter), BF16),
            pltpu.VMEM((tokens, span), BF16),
            pltpu.VMEM((n_tp, tokens // n_tp, model), BF16),
            pltpu.VMEM((n_tp, tokens // n_tp, model), BF16),
            *line,
            *line,
            *line,
            *grid_sem,
            *line_sem,
            *grid_sem,
            *pair,
            *pair,
            *pair,
            dma((max(6, n_tp), nz)),
            dma((max(6, n_tp), nz)),
            *pair,
            dma((n_tp,)),
            dma((n_tp,)),
            dma((4,)),
        ],
        compiler_params=pltpu.CompilerParams(
            collective_id=0, has_side_effects=True, vmem_limit_bytes=67043328
        ),
        name="layer",
    )(
        queries,
        keys,
        values,
        head_lambda,
        head_gain.reshape(1, -1),
        token_rows,
        norm_gain.reshape(1, -1),
        expert_ids.T,
        route_weights.T,
        out_weight,
        gate_weight[0],
        up_weight[0],
        down_weight[0],
    )
    return mixed_rows.astype(BF16), mixed_experts.astype(BF16)


def solution(mesh):
    placed = (
        P("ep", "tp", None),
        P("ep", "tp", None),
        P("ep", "tp", None),
        P("tp"),
        P(),
        P("tp", None),
        P("ep", None),
        P(),
        P("ep", None),
        P("ep", None),
        P("ep", None, "tp"),
        P("ep", None, "tp"),
        P("ep", "tp", None),
    )
    return jax.shard_map(
        body,
        mesh=mesh,
        in_specs=placed,
        out_specs=(P(("ep", "tp"), None), P("ep", "tp")),
        check_vma=False,
    )
```

profile of v0, /device:TPU:0, one launch (start us, length us, event | category | flops | bytes accessed | tf_op | source)
XLA Modules:
  0.0 81.4 jit_solution(3195699015311623146)
XLA Ops:
  0.6 1.6 %copy.21 = bf16[16,8,4,128]{3,1,2,0:T(8,128)(2,1)} copy(bf16[16,8,4,128]{3,2,1,0:T(4,128)(2,1)} %bitcast.21) | data formatting | bytes 262144
  2.2 1.7 %copy_bitcast_fusion = (bf16[128,512]{1,0:T(8,128)(2,1)}, bf16[128,512]{1,0:T(8,128)(2,1)}) fusion(bf16[16,8,4,128]{3,2,1,0:T(4,128)(2,1)} %bitcast.22, bf16[16,8,4,128]{3,2,1,0:T(4,128)(2,1)} %bitcast.23), kind=kLoop, calls=%fused_computation | loop fusion | bytes 524288 | tf_op jit(solution)/shard_map/reshape | solution.py:578
  3.9 74.3 %layer.1 = (f32[32,2048]{1,0:T(8,128)}, f32[128,512]{1,0:T(8,128)}) custom-call(bf16[128,512]{1,0:T(8,128)(2,1)} %bitcast.20, bf16[128,512]{1,0:T(8,128)(2,1)} %get-tuple-element.7.k_ref, bf16[128,512]{1,0:T(8,128)(2,1)} %get-tuple-element.6.v_ref, f32[4]{0:T(128)} %lam_ref.1, f32[1,128]{1,0:T(1,128)} %bitcast.27, bf16[128,2048]{1,0:T(8,128)(2,1)} %rows_ref.1, ...), custom_call_target="tpu_custom_call" | custom-call | tf_op jit(solution)/shard_map/layer/pallas_call | solution.py:587
  78.2 1.6 %convert_element_type.6 = bf16[32,2048]{1,0:T(8,128)(2,1)} convert(f32[32,2048]{1,0:T(8,128)} %get-tuple-element.4) | non-fusion elementwise | flops 65536 | bytes 393216 | tf_op jit(solution)/shard_map/convert_element_type | solution.py:648
  79.8 1.6 %convert_element_type.7 = bf16[128,512]{1,0:T(8,128)(2,1)} convert(f32[128,512]{1,0:T(8,128)} %get-tuple-element.5) | non-fusion elementwise | flops 65536 | bytes 393216 | tf_op jit(solution)/shard_map/convert_element_type | solution.py:648
where the time goes:
time: 81.7 us; the launch traced here: 81.4 us
  Pallas kernels  74.3 us (91%)
  local copies, waits for them, and re-layouts  3.27 us (4%)
  other arithmetic  3.24 us (4%)
    pallas_call x1, Pallas kernels, body(): pl.pallas_call(functools.partial(kernel, n_ep, n_tp, routes, width // 2),...  74.3 us
    convert_element_type x2, other arithmetic, body(): return (mixed_rows.astype(BF16), mixed_experts.astype(BF16))  3.24 us
    reshape x1, local copies, waits for them, and re-layouts, body(): values = value_rows.reshape(tokens, span)  1.69 us

commit v1 on v0

--- a/solution.py
+++ b/solution.py
@@ -31,6 +31,7 @@
     n_tp,
     route_count,
     head_width,
+    by_head,
     q_ref,
     k_ref,
     v_ref,
@@ -50,17 +51,19 @@
     wg,
     wu,
     wd,
-    xfull,
     xb,
     meta,
+    own,
     kvb,
+    hsend,
+    hrecv,
+    split,
     act,
     cbuf,
     pbuf,
     rbuf,
     ubuf,
     vbuf,
-    head_rows,
     prod,
     abuf,
     xs_s,
@@ -85,6 +88,8 @@
     r_r,
     v_s,
     v_r,
+    e_s,
+    e_r,
     a_s,
     a_r,
     w_sem,
@@ -98,6 +103,8 @@
     tokens, model = rows_ref.shape
     quarter = model // n_tp
     hidden = wg.shape[1]
+    width = 2 * head_width
+    heads = q_ref.shape[0] // tokens
 
     weight_copies = [
         pltpu.make_async_copy(src, dst, w_sem.at[i])
@@ -121,13 +128,11 @@
 
     rows = rows_ref[...].astype(F32)
     mean_sq = jnp.mean(rows * rows, axis=-1, keepdims=True)
-    xfull[...] = (rows * lax.rsqrt(mean_sq + NORM_EPS) * norm_gain_ref[...]).astype(BF16)
-    xb[tp, ep] = xfull[:, pl.ds(pl.multiple_of(tp * quarter, quarter), quarter)]
+    normed = (rows * lax.rsqrt(mean_sq + NORM_EPS) * norm_gain_ref[...]).astype(BF16)
+    for j in range(n_tp):
+        xb[j, ep] = normed[:, j * quarter : (j + 1) * quarter]
     meta[ep, :route_count] = ids_ref[...].astype(F32)
     meta[ep, route_count : 2 * route_count] = route_ref[...]
-    span_all = k_ref.shape[1]
-    kvb[ep, :, :span_all] = k_ref[...]
-    kvb[ep, :, span_all:] = v_ref[...]
 
     pl.semaphore_wait(barrier, 1 + (nz - 1) + (n_tp - 1))
 
@@ -185,49 +190,91 @@
         block = xb.at[across, zo * CORES + core, halves[n]]
         return remote(block, block, h_s.at[n, zo], h_r.at[n, zo], ep, targets[n])
 
+    def pair_copy(j, zo, mine=True):
+        block = xb.at[j, zo * CORES + (core if mine else 1 - core)]
+        return remote(block, block, d_s.at[j, zo], d_r.at[j, zo], partner, tp)
+
+    def pair_block(buf, send, recv, zo, mine=True):
+        block = buf.at[zo * CORES + (core if mine else 1 - core)]
+        return remote(block, block, send.at[zo], recv.at[zo], partner, tp)
+
+    start = lambda copy: copy.start()
+
+    def take_x(zo):
+        line_copy(x_own, xs_s, xs_r, zo, 0).wait_recv()
+        each_line(x_own, xs_s, xs_r, zo, start)
+        for n in range(len(targets)):
+            tp_copy(zo, n).start()
+        pair_copy(tp, zo).start()
+        line_copy(meta, ms_s, ms_r, zo, 0).wait_recv()
+        each_line(meta, ms_s, ms_r, zo, start)
+        pair_block(meta, md_s, md_r, zo).start()
+
+    def take_round(r):
+        @pl.when(z + r < nz)
+        def _():
+            take_x(z + r)
+
+        @pl.when(z - r >= 0)
+        def _():
+            take_x(z - r)
+
     def take_tp(zo):
-        for n, j in enumerate(targets):
+        for n in range(len(targets)):
             tp_arrival(zo, n).wait_recv()
         if square:
             for n in range(2):
                 pass_copy(zo, n).start()
-        for n, j in enumerate(targets):
+        for j in targets:
             pair_copy(j, zo).start()
 
-    def pair_copy(j, zo, mine=True):
-        block = xb.at[j, zo * CORES + (core if mine else 1 - core)]
-        return remote(block, block, d_s.at[j, zo], d_r.at[j, zo], partner, tp)
-
-    def pair_block(buf, send, recv, zo, mine=True):
-        block = buf.at[zo * CORES + (core if mine else 1 - core)]
-        return remote(block, block, send.at[zo], recv.at[zo], partner, tp)
-
-    start = lambda copy: copy.start()
-
-    def spread_x(zo):
-        each_line(x_own, xs_s, xs_r, zo, start)
-        for n in range(len(targets)):
-            tp_copy(zo, n).start()
-        pair_copy(tp, zo).start()
-        each_line(meta, ms_s, ms_r, zo, start)
-        pair_block(meta, md_s, md_r, zo).start()
+    def take_pass(zo):
+        if square:
+            for n in range(2):
+                pass_arrival(zo, n).wait_recv()
+            pair_copy(across, zo).start()
+
+    def take_pair(zo):
+        for j in range(n_tp):
+            pair_copy(j, zo, False).wait_recv()
+        pair_block(meta, md_s, md_r, zo, False).wait_recv()
 
     def spread_kv(zo):
         each_line(kvb, ks_s, ks_r, zo, start)
         pair_block(kvb, kd_s, kd_r, zo).start()
 
-    def take_x(zo):
-        line_copy(x_own, xs_s, xs_r, zo, 0).wait_recv()
-        line_copy(meta, ms_s, ms_r, zo, 0).wait_recv()
-        spread_x(zo)
-
     def take_kv(zo):
         line_copy(kvb, ks_s, ks_r, zo, 0).wait_recv()
         spread_kv(zo)
 
-    def half_copy(zo):
-        return remote(
-            cbuf.at[zo, 1 - core], pbuf.at[zo], p_s.at[zo], p_r.at[zo], partner, tp
+    def head_copy(zo):
+        return remote(
+            own.at[zo], kvb.at[ep], ks_s.at[0, zo], ks_r.at[z], zo * CORES + core, tp
+        )
+
+    def head_arrival(zo):
+        block = kvb.at[zo * CORES + core]
+        return remote(block, block, ks_s.at[0, zo], ks_r.at[zo], zo * CORES + core, tp)
+
+    def head_pair(zo, mine=True):
+        block = kvb.at[zo * CORES + (core if mine else 1 - core), pl.ds(1, 2)]
+        return remote(block, block, kd_s.at[zo], kd_r.at[zo], partner, tp)
+
+    def back_copy(zo):
+        return remote(
+            hsend.at[zo], hrecv.at[z], e_s.at[zo], e_r.at[z], zo * CORES + core, tp
+        )
+
+    def back_arrival(zo):
+        return remote(
+            hsend.at[zo], hrecv.at[zo], e_s.at[zo], e_r.at[zo], zo * CORES + core, tp
+        )
+
+    order = [across, side, other, tp] if square else [(tp + off) % n_tp for off in range(1, n_tp + 1)]
+
+    def half_copy(zo, j):
+        return remote(
+            cbuf.at[zo, 1 - core, j], pbuf.at[zo, j], p_s.at[j, zo], p_r.at[j, zo], partner, tp
         )
 
     def term_parts():
@@ -273,11 +320,20 @@
             device,
         )
 
+    def finish(zo):
+        sends = {0: (1, 3), 1: (0,), 2: (2,)} if square else {i: (i,) for i in range(n_tp - 1)}
+        for i, j in enumerate(order):
+            half_copy(zo, j).wait_recv()
+            cbuf[zo, core, j] = (
+                cbuf[zo, core, j].astype(F32) + pbuf[zo, j].astype(F32)
+            ).astype(BF16)
+            for n in sends.get(i, ()):
+                term_copy(zo, n).start()
+
     def middle(zo):
         if square:
-            for n in range(4):
-                term_arrival(zo, n).wait_recv()
-            for n, j in ((4, other), (5, side)):
+            for n, arrived, j in ((4, 1, other), (5, 3, side)):
+                term_arrival(zo, arrived).wait_recv()
                 rows_of = halves[n - 4]
                 cbuf[zo, core, j, rows_of] = (
                     cbuf[zo, core, j, rows_of].astype(F32) + rbuf[zo, j, rows_of].astype(F32)
@@ -294,19 +350,10 @@
             ubuf.at[zo], vbuf.at[zo], v_s.at[zo], v_r.at[zo], zo * CORES + core, tp
         )
 
-    def finish(zo):
-        half_copy(zo).wait_recv()
-        for j in range(n_tp):
-            cbuf[zo, core, j] = (
-                cbuf[zo, core, j].astype(F32) + pbuf[zo, j].astype(F32)
-            ).astype(BF16)
-        for n in range(4 if square else len(targets)):
-            term_copy(zo, n).start()
-
     def reduce(zo):
         total = cbuf[zo, core, tp].astype(F32)
         if square:
-            for n in (4, 5):
+            for n in (0, 2, 4, 5):
                 term_arrival(zo, n).wait_recv()
             total = total + rbuf[zo, tp].astype(F32) + rbuf[zo, across].astype(F32)
         else:
@@ -320,43 +367,29 @@
             home_copy(zo).start()
 
     tile = min(256, hidden)
-
-    def experts(i, zo):
+    tiles = hidden // tile
+
+    def hidden_tile(zo, f):
         pair = pl.ds(zo * CORES, CORES)
-
-        def hidden_tile(f, carry):
-            cols = pl.ds(pl.multiple_of(f * tile, tile), tile)
-            gate = jnp.zeros((CORES * tokens, tile), F32)
-            up = jnp.zeros((CORES * tokens, tile), F32)
-            for j in range(n_tp):
-                chunk = xb[j, pair].reshape(CORES * tokens, quarter)
-                depth = pl.ds(j * quarter, quarter)
-                gate = gate + jnp.dot(chunk, wg[depth, cols], preferred_element_type=F32)
-                up = up + jnp.dot(chunk, wu[depth, cols], preferred_element_type=F32)
-            gated = jnp.minimum(gate, CLAMP_LIMIT)
-            clipped = jnp.clip(up, -CLAMP_LIMIT, CLAMP_LIMIT)
-            act[:, cols] = (
-                (clipped + 1.0) * gated * jax.nn.sigmoid(GATE_SLOPE * gated)
-            ).astype(BF16)
-            return carry
-
-        lax.fori_loop(0, hidden // tile, hidden_tile, 0)
-
-        @pl.when(i > 1)
-        def _():
-            middle(origin(i - 2))
-
-        @pl.when(i + 1 < nz)
-        def _():
-            take_tp(origin(i + 1))
-
-        @pl.when(i > 0)
-        def _():
-            finish(origin(i - 1))
-
-        eye = lax.broadcasted_iota(jnp.int32, (tokens, tokens), 0) == lax.broadcasted_iota(
-            jnp.int32, (tokens, tokens), 1
-        )
+        cols = pl.ds(f * tile, tile)
+        gate = jnp.zeros((CORES * tokens, tile), F32)
+        up = jnp.zeros((CORES * tokens, tile), F32)
+        for j in range(n_tp):
+            chunk = xb[j, pair].reshape(CORES * tokens, quarter)
+            depth = pl.ds(j * quarter, quarter)
+            gate = gate + jnp.dot(chunk, wg[depth, cols], preferred_element_type=F32)
+            up = up + jnp.dot(chunk, wu[depth, cols], preferred_element_type=F32)
+        gated = jnp.minimum(gate, CLAMP_LIMIT)
+        clipped = jnp.clip(up, -CLAMP_LIMIT, CLAMP_LIMIT)
+        act[:, cols] = (
+            (clipped + 1.0) * gated * jax.nn.sigmoid(GATE_SLOPE * gated)
+        ).astype(BF16)
+
+    eye = lax.broadcasted_iota(jnp.int32, (tokens, tokens), 0) == lax.broadcasted_iota(
+        jnp.int32, (tokens, tokens), 1
+    )
+
+    def route_scale(zo):
         columns = []
         for c in range(CORES):
             info = meta[zo * CORES + c]
@@ -364,51 +397,95 @@
             weights = jnp.where(named, info[route_count : 2 * route_count], 0.0)
             line = jnp.sum(weights, axis=0, keepdims=True)
             columns.append(jnp.sum(jnp.where(eye, line, 0.0), axis=1, keepdims=True))
-        scale = jnp.concatenate(columns, axis=0)
-
-        def model_tile(j, carry):
-            cols = pl.ds(pl.multiple_of(j * quarter, quarter), quarter)
-            value = jnp.dot(act[...], wd[:, cols], preferred_element_type=F32) * scale
-            value = value.astype(BF16)
-            for c in range(CORES):
-                cbuf[zo, c, j] = value[c * tokens : (c + 1) * tokens]
-            return carry
-
-        lax.fori_loop(0, n_tp, model_tile, 0)
-        half_copy(zo).start()
-
-    spread_x(z)
-    take_tp(z)
+        return jnp.concatenate(columns, axis=0)
+
+    def model_tile(zo, j, scale):
+        cols = pl.ds(pl.multiple_of(j * quarter, quarter), quarter)
+        value = jnp.dot(act[...], wd[:, cols], preferred_element_type=F32) * scale
+        value = value.astype(BF16)
+        for c in range(CORES):
+            cbuf[zo, c, j] = value[c * tokens : (c + 1) * tokens]
+        half_copy(zo, j).start()
+
+    each_line(x_own, xs_s, xs_r, z, start)
+    for j in range(n_tp):
+        pair_copy(j, z).start()
+    each_line(meta, ms_s, ms_r, z, start)
+    pair_block(meta, md_s, md_r, z).start()
+
+    for part, ref in enumerate((q_ref, k_ref, v_ref)):
+        split[...] = ref[...].astype(F32)
+        for h in range(heads):
+            own[h, part] = split[pl.ds(h, tokens, stride=heads), :].astype(BF16)
+    if by_head:
+        kvb[ep] = own[z]
+        head_pair(z).start()
+    else:
+        for h in range(heads):
+            for part in range(2):
+                at = (part * heads + h) * width
+                kvb[ep, :, at : at + width] = own[h, 1 + part]
 
     def step(i, carry):
         zo = origin(i)
-
-        @pl.when(i + 1 < nz)
-        def _():
-            take_x(origin(i + 1))
+        take_pair(zo)
 
         @pl.when(i == 0)
         def _():
-            spread_kv(z)
-
-        @pl.when(i > 0)
-        def _():
-            take_kv(zo)
-
-        if square:
-            for n in range(2):
-                pass_arrival(zo, n).wait_recv()
-            pair_copy(across, zo).start()
-        for j in range(n_tp):
-            pair_copy(j, zo, False).wait_recv()
-        pair_block(meta, md_s, md_r, zo, False).wait_recv()
+            for copy in weight_copies[:2]:
+                copy.wait()
+
+        for f in range(tiles):
+            hidden_tile(zo, f)
+            if f == min(1, tiles - 1):
+
+                @pl.when(i == 0)
+                def _():
+                    take_round(1)
+
+                @pl.when(i > 1)
+                def _():
+                    middle(origin(i - 2))
+
+                @pl.when(i > 0)
+                def _():
+                    finish(origin(i - 1))
+
+        @pl.when((i > 0) & (i + 1 < nz))
+        def _():
+            take_pass(origin(i + 1))
 
         @pl.when(i == 0)
         def _():
-            for copy in weight_copies[:3]:
-                copy.wait()
-
-        experts(i, zo)
+            weight_copies[2].wait()
+
+        scale = route_scale(zo)
+        for j in order:
+            model_tile(zo, j, scale)
+
+        @pl.when(i == 0)
+        def _():
+            take_round(2)
+            if by_head:
+                for off in range(1, nz):
+                    head_copy((z + off) % nz).start()
+            else:
+                spread_kv(z)
+            if nz > 1:
+                take_tp(origin(1))
+                take_pass(origin(1))
+
+        if not by_head:
+
+            @pl.when(i > 0)
+            def _():
+                take_kv(zo)
+
+        take_round(i + 3)
+
+        @pl.when(i + 2 < nz)
+        def _():
+            take_tp(origin(i + 2))
 
         @pl.when(i > 1)
         def _():
@@ -418,33 +495,60 @@
 
     lax.fori_loop(0, nz, step, 0)
 
-    def wait_kv(i, carry):
-        pair_block(kvb, kd_s, kd_r, i, False).wait_recv()
-        return carry
-
-    lax.fori_loop(0, nz, wait_kv, 0)
+    if by_head:
+        for off in range(1, nz):
+            zs = (z + off) % nz
+            head_arrival(zs).wait_recv()
+            head_pair(zs).start()
+    finish(origin(nz - 1))
     middle(origin(nz - 2))
-    finish(origin(nz - 1))
-
-    width = 2 * head_width
-    all_heads = q_ref.shape[1]
-    heads = all_heads // width
+
+    gain = gain_ref[...]
+    lane = lax.broadcasted_iota(jnp.int32, (tokens, width), 1)
+
+    def both_maps(query):
+        nothing = jnp.zeros_like(query)
+        return jnp.concatenate(
+            [jnp.where(lane < head_width, query, nothing), jnp.where(lane < head_width, nothing, query)],
+            axis=0,
+        )
+
+    def head_norm(value_sum, total, lam):
+        mean = value_sum / total
+        attended = mean[:tokens] - lam * mean[tokens:]
+        mean_sq = jnp.mean(attended * attended, axis=-1, keepdims=True)
+        return (attended * lax.rsqrt(mean_sq + NORM_EPS) * gain).astype(BF16)
+
+    def position_block(n):
+        at = n * CORES + core
+        extent = (n + 1) * CORES * tokens
+        keys = kvb[: (n + 1) * CORES, 1].reshape(extent, width)
+        values = kvb[: (n + 1) * CORES, 2].reshape(extent, width)
+        score = lax.dot_general(
+            both_maps(kvb[at, 0]), keys, (((1,), (1,)), ((), ())), preferred_element_type=F32
+        ) * (head_width**-0.5)
+        row = lax.broadcasted_iota(jnp.int32, (2 * tokens, extent), 0) % tokens + at * tokens
+        col = lax.broadcasted_iota(jnp.int32, (2 * tokens, extent), 1)
+        score = jnp.where(col <= row, score, -1e30)
+        terms = jnp.exp(score - jnp.max(score, axis=1, keepdims=True))
+        total = jnp.sum(terms, axis=1, keepdims=True)
+        value_sum = jnp.dot(terms.astype(BF16), values, preferred_element_type=F32)
+        result = head_norm(value_sum, total, lam_ref[z])
+        hsend[n] = result
+
+        @pl.when(z != n)
+        def _():
+            back_copy(n).start()
+
     key_blocks = min(n_ep, 8)
     key_span = key_blocks * tokens
-    lane = lax.broadcasted_iota(jnp.int32, (tokens, width), 1)
-    gain = gain_ref[...]
 
     def one_head(h, carry):
-        cols = pl.ds(pl.multiple_of(h * width, width), width)
-        value_cols = pl.ds(pl.multiple_of(all_heads + h * width, width), width)
-        query = q_ref[:, cols]
-        nothing = jnp.zeros_like(query)
-        both = jnp.concatenate(
-            [jnp.where(lane < head_width, query, nothing), jnp.where(lane < head_width, nothing, query)],
-            axis=0,
-        )
+        both = both_maps(own[h, 0])
         row = lax.broadcasted_iota(jnp.int32, (2 * tokens, key_span), 0) % tokens + ep * tokens
         col = lax.broadcasted_iota(jnp.int32, (2 * tokens, key_span), 1)
+        cols = pl.ds(pl.multiple_of(h * width, width), width)
+        value_cols = pl.ds(pl.multiple_of((heads + h) * width, width), width)
 
         def span(s, state):
             top, total, value_sum = state
@@ -469,31 +573,40 @@
             jnp.zeros((2 * tokens, 1), F32),
             jnp.zeros((2 * tokens, width), F32),
         )
-        if n_ep == key_blocks:
-            state = span(0, state)
-        else:
-            state = lax.fori_loop(0, n_ep // key_blocks, span, state)
-        mean = state[2] / state[1]
-        attended = mean[:tokens] - lam_ref[h] * mean[tokens:]
-        mean_sq = jnp.mean(attended * attended, axis=-1, keepdims=True)
-        head_rows[:, cols] = (attended * lax.rsqrt(mean_sq + NORM_EPS) * gain).astype(BF16)
+        state = lax.fori_loop(0, n_ep // key_blocks, span, state)
+        hsend[h] = head_norm(state[2], state[1], lam_ref[h])
         return carry
 
-    lax.fori_loop(0, heads // 2, one_head, 0)
-    middle(origin(nz - 1))
-    reduce(origin(nz - 2))
-    lax.fori_loop(heads // 2, heads, one_head, 0)
+    if by_head:
+        for n in range(nz):
+            head_pair(n, False).wait_recv()
+        for n in range(nz):
+            position_block(n)
+        hrecv[z] = hsend[z]
+        reduce(origin(nz - 2))
+        middle(origin(nz - 1))
+        for off in range(1, nz):
+            back_arrival((z + off) % nz).wait_recv()
+        head_rows = jnp.concatenate([hrecv[h] for h in range(heads)], axis=1)
+    else:
+
+        def wait_kv(i, carry):
+            pair_block(kvb, kd_s, kd_r, i, False).wait_recv()
+            return carry
+
+        lax.fori_loop(0, nz, wait_kv, 0)
+        lax.fori_loop(0, heads, one_head, 0)
+        reduce(origin(nz - 2))
+        middle(origin(nz - 1))
+        head_rows = jnp.concatenate([hsend[h] for h in range(heads)], axis=1)
     weight_copies[3].wait()
     out_rows = tokens // n_tp
 
-    def product_tile(n, carry):
-        cols = pl.ds(pl.multiple_of(n * quarter, quarter), quarter)
-        value = jnp.dot(head_rows[...], ow[:, cols], preferred_element_type=F32).astype(BF16)
+    for n in range(n_tp):
+        cols = pl.ds(n * quarter, quarter)
+        value = jnp.dot(head_rows, ow[:, cols], preferred_element_type=F32).astype(BF16)
         for j in range(n_tp):
             prod[j, :, cols] = value[j * out_rows : (j + 1) * out_rows]
-        return carry
-
-    lax.fori_loop(0, n_tp, product_tile, 0)
 
     def row_copy(off):
         j = (tp + off) % n_tp
@@ -525,23 +638,29 @@
     def drain(zo, carry):
         each_line(x_own, xs_s, xs_r, zo, left)
         each_line(meta, ms_s, ms_r, zo, left)
-        each_line(kvb, ks_s, ks_r, zo, left)
-        for n in range(len(targets)):
-            tp_copy(zo, n).wait_send()
         for n in range(len(term_parts())):
             term_copy(zo, n).wait_send()
-        if square:
-            for n in range(2):
-                pass_copy(zo, n).wait_send()
         for j in range(n_tp):
             pair_copy(j, zo).wait_send()
+            half_copy(zo, j).wait_send()
         pair_block(meta, md_s, md_r, zo).wait_send()
-        pair_block(kvb, kd_s, kd_r, zo).wait_send()
-        half_copy(zo).wait_send()
+        if by_head:
+            head_pair(zo).wait_send()
+        else:
+            each_line(kvb, ks_s, ks_r, zo, left)
+            pair_block(kvb, kd_s, kd_r, zo).wait_send()
 
         @pl.when(zo != z)
         def _():
             home_copy(zo).wait_send()
+            for n in range(len(targets)):
+                tp_copy(zo, n).wait_send()
+            if square:
+                for n in range(2):
+                    pass_copy(zo, n).wait_send()
+            if by_head:
+                head_copy(zo).wait_send()
+                back_copy(zo).wait_send()
 
         return carry
 
@@ -573,9 +692,8 @@
     hidden = gate_weight.shape[2]
     routes = expert_ids.shape[1]
     span = heads * width
-    queries = query_maps.reshape(tokens, span)
-    keys = key_maps.reshape(tokens, span)
-    values = value_rows.reshape(tokens, span)
+    by_head = heads == nz
+    flat = (tokens * heads, width)
     vmem = pl.BlockSpec(memory_space=pltpu.VMEM)
     smem = pl.BlockSpec(memory_space=pltpu.SMEM)
     hbm = pl.BlockSpec(memory_space=pltpu.HBM)
@@ -585,7 +703,7 @@
     grid_sem = [dma((n_tp, nz)), dma((n_tp, nz))]
     pair = [dma((nz,)), dma((nz,))]
     mixed_rows, mixed_experts = pl.pallas_call(
-        functools.partial(kernel, n_ep, n_tp, routes, width // 2),
+        functools.partial(kernel, n_ep, n_tp, routes, width // 2, by_head),
         out_shape=(
             jax.ShapeDtypeStruct((tokens // n_tp, model), F32),
             jax.ShapeDtypeStruct((tokens, quarter), F32),
@@ -597,17 +715,19 @@
             pltpu.VMEM((model, hidden), BF16),
             pltpu.VMEM((model, hidden), BF16),
             pltpu.VMEM((hidden, model), BF16),
-            pltpu.VMEM((tokens, model), BF16),
             pltpu.VMEM((n_tp, n_ep, tokens, quarter), BF16),
             pltpu.VMEM((n_ep, 2 * routes, tokens), F32),
-            pltpu.VMEM((n_ep, tokens, 2 * span), BF16),
+            pltpu.VMEM((heads, 3, tokens, width), BF16),
+            pltpu.VMEM((n_ep, 3, tokens, width) if by_head else (n_ep, tokens, 2 * span), BF16),
+            pltpu.VMEM((heads, tokens, width), BF16),
+            pltpu.VMEM((heads, tokens, width), BF16),
+            pltpu.VMEM(flat, F32),
             pltpu.VMEM((CORES * tokens, hidden), BF16),
             pltpu.VMEM((nz, CORES, n_tp, tokens, quarter), BF16),
             pltpu.VMEM((nz, n_tp, tokens, quarter), BF16),
             pltpu.VMEM((nz, n_tp, tokens, quarter), BF16),
             pltpu.VMEM((nz, tokens, quarter), BF16),
             pltpu.VMEM((nz, tokens, quarter), BF16),
-            pltpu.VMEM((tokens, span), BF16),
             pltpu.VMEM((n_tp, tokens // n_tp, model), BF16),
             pltpu.VMEM((n_tp, tokens // n_tp, model), BF16),
             *line,
@@ -618,9 +738,10 @@
             *grid_sem,
             *pair,
             *pair,
-            *pair,
+            *grid_sem,
             dma((max(6, n_tp), nz)),
             dma((max(6, n_tp), nz)),
+            *pair,
             *pair,
             dma((n_tp,)),
             dma((n_tp,)),
@@ -631,9 +752,9 @@
         ),
         name="layer",
     )(
-        queries,
-        keys,
-        values,
+        query_maps.reshape(flat),
+        key_maps.reshape(flat),
+        value_rows.reshape(flat),
         head_lambda,
         head_gain.reshape(1, -1),
         token_rows,

time: 81.7 us -> 65.5 us (0.80)
  Pallas kernels: 74.3 us -> 61.4 us
  local copies, waits for them, and re-layouts: 3.27 us -> 0 us
    pallas_call x1, Pallas kernels: 74.3 us -> 61.4 us  [body(): pl.pallas_call(functools.partial(kernel, n_ep, n_tp, routes, width // 2,...]
    reshape x1 -> x0, local copies, waits for them, and re-layouts: 1.69 us -> none  [body(): values = value_rows.reshape(tokens, span)]
    unnamed x1 -> x0, local copies, waits for them, and re-layouts: 1.58 us -> none
where the time goes in v1:
time: 65.5 us; the launch traced here: 65.3 us
  Pallas kernels  61.4 us (94%)
  other arithmetic  3.24 us (5%)
    pallas_call x1, Pallas kernels, body(): pl.pallas_call(functools.partial(kernel, n_ep, n_tp, routes, width // 2,...  61.4 us
    convert_element_type x2, other arithmetic, body(): return (mixed_rows.astype(BF16), mixed_experts.astype(BF16))  3.24 us

profile of v1, /device:TPU:0, one launch (start us, length us, event | category | flops | bytes accessed | tf_op | source)
XLA Modules:
  0.0 65.3 jit_solution(16012247053687975029)
XLA Ops:
  0.6 61.4 %layer.1 = (f32[32,2048]{1,0:T(8,128)}, f32[128,512]{1,0:T(8,128)}) custom-call(bf16[512,128]{1,0:T(8,128)(2,1)} %bitcast.13, bf16[512,128]{1,0:T(8,128)(2,1)} %bitcast.14, bf16[512,128]{1,0:T(8,128)(2,1)} %bitcast.15, f32[4]{0:T(128)} %lam_ref.1, f32[1,128]{1,0:T(1,128)} %bitcast.19, bf16[128,2048]{1,0:T(8,128)(2,1)} %rows_ref.1, f32[1,2048]{1,0:T(1,128)} %bitcast.16, ...), custom_call_target="tpu_custom_call" | custom-call | tf_op jit(solution)/shard_map/layer/pallas_call | solution.py:705
  62.0 1.6 %convert_element_type.6 = bf16[32,2048]{1,0:T(8,128)(2,1)} convert(f32[32,2048]{1,0:T(8,128)} %get-tuple-element.4) | non-fusion elementwise | flops 65536 | bytes 393216 | tf_op jit(solution)/shard_map/convert_element_type | solution.py:769
  63.6 1.6 %convert_element_type.7 = bf16[128,512]{1,0:T(8,128)(2,1)} convert(f32[128,512]{1,0:T(8,128)} %get-tuple-element.5) | non-fusion elementwise | flops 65536 | bytes 393216 | tf_op jit(solution)/shard_map/convert_element_type | solution.py:769

commit v2 on v1

--- a/solution.py
+++ b/solution.py
@@ -32,6 +32,21 @@
     route_count,
     head_width,
     by_head,
+    q_hbm,
+    k_hbm,
+    v_hbm,
+    lam_hbm,
+    gain_hbm,
+    rows_hbm,
+    norm_gain_hbm,
+    ids_hbm,
+    route_hbm,
+    ow_hbm,
+    wg_hbm,
+    wu_hbm,
+    wd_hbm,
+    out_rows_ref,
+    out_exp_ref,
     q_ref,
     k_ref,
     v_ref,
@@ -41,12 +56,6 @@
     norm_gain_ref,
     ids_ref,
     route_ref,
-    ow_hbm,
-    wg_hbm,
-    wu_hbm,
-    wd_hbm,
-    out_rows_ref,
-    out_exp_ref,
     ow,
     wg,
     wu,
@@ -92,6 +101,7 @@
     e_r,
     a_s,
     a_r,
+    i_sem,
     w_sem,
 ):
     nz = n_ep // CORES
@@ -106,13 +116,6 @@
     width = 2 * head_width
     heads = q_ref.shape[0] // tokens
 
-    weight_copies = [
-        pltpu.make_async_copy(src, dst, w_sem.at[i])
-        for i, (src, dst) in enumerate([(wg_hbm, wg), (wu_hbm, wu), (wd_hbm, wd), (ow_hbm, ow)])
-    ]
-    for copy in weight_copies:
-        copy.start()
-
     barrier = pltpu.get_barrier_semaphore()
 
     def greet(e, t):
@@ -125,6 +128,29 @@
         greet(((z + off) % nz) * CORES + core, tp)
     for off in range(1, n_tp):
         greet(ep, (tp + off) % n_tp)
+
+    inputs = [
+        (rows_hbm, rows_ref),
+        (norm_gain_hbm, norm_gain_ref),
+        (ids_hbm, ids_ref),
+        (route_hbm, route_ref),
+        (q_hbm, q_ref),
+        (k_hbm, k_ref),
+        (v_hbm, v_ref),
+        (lam_hbm, lam_ref),
+        (gain_hbm, gain_ref),
+    ]
+    input_copies = [
+        pltpu.make_async_copy(src, dst, i_sem.at[i]) for i, (src, dst) in enumerate(inputs)
+    ]
+    weight_copies = [
+        pltpu.make_async_copy(src, dst, w_sem.at[i])
+        for i, (src, dst) in enumerate([(wg_hbm, wg), (wu_hbm, wu), (wd_hbm, wd), (ow_hbm, ow)])
+    ]
+    for copy in input_copies + weight_copies:
+        copy.start()
+    for copy in input_copies[:4]:
+        copy.wait()
 
     rows = rows_ref[...].astype(F32)
     mean_sq = jnp.mean(rows * rows, axis=-1, keepdims=True)
@@ -154,7 +180,25 @@
             tp,
         )
 
-    x_own = xb.at[tp]
+    def x_line(zo, h, way):
+        block = xb.at[tp, zo * CORES + core, halves[h]]
+        return remote(
+            block,
+            block,
+            xs_s.at[way * 2 + h, zo],
+            xs_r.at[h, zo],
+            (z + (1 if way == 0 else -1)) * CORES + core,
+            tp,
+        )
+
+    def each_x(zo, h, act_on):
+        @pl.when((zo <= z) & (z < nz - 1))
+        def _():
+            act_on(x_line(zo, h, 0))
+
+        @pl.when((zo >= z) & (z > 0))
+        def _():
+            act_on(x_line(zo, h, 1))
 
     def each_line(buf, send, recv, zo, act_on):
         @pl.when((zo <= z) & (z < nz - 1))
@@ -173,14 +217,15 @@
     halves = (pl.ds(0, half), pl.ds(half, half))
     targets = [side, other] if square else [(tp + off) % n_tp for off in range(1, n_tp)]
 
-    def tp_copy(zo, n):
-        block = xb.at[tp, zo * CORES + core]
-        return remote(block, block, t_s.at[n, zo], t_r.at[tp, zo], ep, targets[n])
-
-    def tp_arrival(zo, n):
+    def tp_copy(zo, n, h):
+        block = xb.at[tp, zo * CORES + core, halves[h]]
+        return remote(block, block, t_s.at[h, n, zo], t_r.at[h, n, zo], ep, targets[n])
+
+    def tp_arrival(zo, n, h):
         j = targets[n]
-        block = xb.at[j, zo * CORES + core]
-        return remote(block, block, t_s.at[n, zo], t_r.at[j, zo], ep, j)
+        block = xb.at[j, zo * CORES + core, halves[h]]
+        k = n if square else len(targets) - 1 - n
+        return remote(block, block, t_s.at[h, n, zo], t_r.at[h, k, zo], ep, j)
 
     def pass_copy(zo, n):
         block = xb.at[other if n == 0 else side, zo * CORES + core, halves[n]]
@@ -200,33 +245,34 @@
 
     start = lambda copy: copy.start()
 
-    def take_x(zo):
-        line_copy(x_own, xs_s, xs_r, zo, 0).wait_recv()
-        each_line(x_own, xs_s, xs_r, zo, start)
+    def take_x(zo, h):
+        x_line(zo, h, 0).wait_recv()
+        each_x(zo, h, start)
         for n in range(len(targets)):
-            tp_copy(zo, n).start()
-        pair_copy(tp, zo).start()
-        line_copy(meta, ms_s, ms_r, zo, 0).wait_recv()
-        each_line(meta, ms_s, ms_r, zo, start)
-        pair_block(meta, md_s, md_r, zo).start()
-
-    def take_round(r):
+            tp_copy(zo, n, h).start()
+        if h == 1:
+            pair_copy(tp, zo).start()
+            line_copy(meta, ms_s, ms_r, zo, 0).wait_recv()
+            each_line(meta, ms_s, ms_r, zo, start)
+            pair_block(meta, md_s, md_r, zo).start()
+
+    def take_round(r, h):
         @pl.when(z + r < nz)
         def _():
-            take_x(z + r)
+            take_x(z + r, h)
 
         @pl.when(z - r >= 0)
         def _():
-            take_x(z - r)
-
-    def take_tp(zo):
+            take_x(z - r, h)
+
+    def take_tp(zo, h):
         for n in range(len(targets)):
-            tp_arrival(zo, n).wait_recv()
+            tp_arrival(zo, n, h).wait_recv()
         if square:
-            for n in range(2):
-                pass_copy(zo, n).start()
-        for j in targets:
-            pair_copy(j, zo).start()
+            pass_copy(zo, h).start()
+        if h == 1:
+            for j in targets:
+                pair_copy(j, zo).start()
 
     def take_pass(zo):
         if square:
@@ -399,109 +445,75 @@
             columns.append(jnp.sum(jnp.where(eye, line, 0.0), axis=1, keepdims=True))
         return jnp.concatenate(columns, axis=0)
 
-    def model_tile(zo, j, scale):
-        cols = pl.ds(pl.multiple_of(j * quarter, quarter), quarter)
-        value = jnp.dot(act[...], wd[:, cols], preferred_element_type=F32) * scale
-        value = value.astype(BF16)
-        for c in range(CORES):
-            cbuf[zo, c, j] = value[c * tokens : (c + 1) * tokens]
-        half_copy(zo, j).start()
-
-    each_line(x_own, xs_s, xs_r, z, start)
+    def model_tiles(zo, places, scale):
+        for j in places:
+            cols = pl.ds(pl.multiple_of(j * quarter, quarter), quarter)
+            value = jnp.dot(act[...], wd[:, cols], preferred_element_type=F32) * scale
+            value = value.astype(BF16)
+            for c in range(CORES):
+                cbuf[zo, c, j] = value[c * tokens : (c + 1) * tokens]
+        for j in places:
+            half_copy(zo, j).start()
+
+    for h in range(2):
+        each_x(z, h, start)
     for j in range(n_tp):
         pair_copy(j, z).start()
     each_line(meta, ms_s, ms_r, z, start)
     pair_block(meta, md_s, md_r, z).start()
 
-    for part, ref in enumerate((q_ref, k_ref, v_ref)):
-        split[...] = ref[...].astype(F32)
-        for h in range(heads):
-            own[h, part] = split[pl.ds(h, tokens, stride=heads), :].astype(BF16)
-    if by_head:
-        kvb[ep] = own[z]
-        head_pair(z).start()
-    else:
-        for h in range(heads):
-            for part in range(2):
-                at = (part * heads + h) * width
-                kvb[ep, :, at : at + width] = own[h, 1 + part]
-
-    def step(i, carry):
-        zo = origin(i)
-        take_pair(zo)
-
-        @pl.when(i == 0)
-        def _():
-            for copy in weight_copies[:2]:
-                copy.wait()
-
-        for f in range(tiles):
-            hidden_tile(zo, f)
-            if f == min(1, tiles - 1):
-
-                @pl.when(i == 0)
-                def _():
-                    take_round(1)
-
-                @pl.when(i > 1)
-                def _():
-                    middle(origin(i - 2))
-
-                @pl.when(i > 0)
-                def _():
-                    finish(origin(i - 1))
-
-        @pl.when((i > 0) & (i + 1 < nz))
-        def _():
-            take_pass(origin(i + 1))
-
-        @pl.when(i == 0)
-        def _():
-            weight_copies[2].wait()
-
-        scale = route_scale(zo)
-        for j in order:
-            model_tile(zo, j, scale)
-
-        @pl.when(i == 0)
-        def _():
-            take_round(2)
-            if by_head:
-                for off in range(1, nz):
-                    head_copy((z + off) % nz).start()
-            else:
-                spread_kv(z)
-            if nz > 1:
-                take_tp(origin(1))
-                take_pass(origin(1))
-
-        if not by_head:
-
-            @pl.when(i > 0)
-            def _():
-                take_kv(zo)
-
-        take_round(i + 3)
-
-        @pl.when(i + 2 < nz)
-        def _():
-            take_tp(origin(i + 2))
-
-        @pl.when(i > 1)
-        def _():
-            reduce(origin(i - 2))
-
-        return carry
-
-    lax.fori_loop(0, nz, step, 0)
-
+    tiles_early = tiles // 2
+    early = len(order) // 2
+
+    def split_heads():
+        for copy in input_copies[4:]:
+            copy.wait()
+        for part, ref in enumerate((q_ref, k_ref, v_ref)):
+            split[...] = ref[...].astype(F32)
+            for h in range(heads):
+                own[h, part] = split[pl.ds(h, tokens, stride=heads), :].astype(BF16)
+        if by_head:
+            kvb[ep] = own[z]
+            head_pair(z).start()
+        else:
+            for h in range(heads):
+                for part in range(2):
+                    at = (part * heads + h) * width
+                    kvb[ep, :, at : at + width] = own[h, 1 + part]
+
+    def in_early(f):
+        if f == 0:
+            take_round(1, 0)
+        if f == tiles - 2:
+            take_round(1, 1)
+
+    take_pair(z)
+    for copy in weight_copies[:2]:
+        copy.wait()
+    for f in range(tiles):
+        hidden_tile(z, f)
+        in_early(f)
+    weight_copies[2].wait()
+    scale = route_scale(z)
+    model_tiles(z, order[:early], scale)
+    take_round(2, 0)
+    take_tp(origin(1), 0)
+    model_tiles(z, order[early:], scale)
+    take_round(2, 1)
+    take_tp(origin(1), 1)
+    take_round(3, 0)
+    if nz > 2:
+        take_tp(origin(2), 0)
+    split_heads()
+    take_round(3, 1)
+    if nz > 2:
+        take_tp(origin(2), 1)
     if by_head:
         for off in range(1, nz):
-            zs = (z + off) % nz
-            head_arrival(zs).wait_recv()
-            head_pair(zs).start()
-    finish(origin(nz - 1))
-    middle(origin(nz - 2))
+            head_copy((z + off) % nz).start()
+    else:
+        spread_kv(z)
+    take_pass(origin(1))
 
     gain = gain_ref[...]
     lane = lax.broadcasted_iota(jnp.int32, (tokens, width), 1)
@@ -512,6 +524,10 @@
             [jnp.where(lane < head_width, query, nothing), jnp.where(lane < head_width, nothing, query)],
             axis=0,
         )
+
+    def lam_of(h):
+        place = lax.broadcasted_iota(jnp.int32, lam_ref.shape, 1)
+        return jnp.sum(jnp.where(place == h, lam_ref[...], 0.0), axis=1, keepdims=True)
 
     def head_norm(value_sum, total, lam):
         mean = value_sum / total
@@ -533,7 +549,7 @@
         terms = jnp.exp(score - jnp.max(score, axis=1, keepdims=True))
         total = jnp.sum(terms, axis=1, keepdims=True)
         value_sum = jnp.dot(terms.astype(BF16), values, preferred_element_type=F32)
-        result = head_norm(value_sum, total, lam_ref[z])
+        result = head_norm(value_sum, total, lam_of(z))
         hsend[n] = result
 
         @pl.when(z != n)
@@ -574,20 +590,86 @@
             jnp.zeros((2 * tokens, width), F32),
         )
         state = lax.fori_loop(0, n_ep // key_blocks, span, state)
-        hsend[h] = head_norm(state[2], state[1], lam_ref[h])
+        hsend[h] = head_norm(state[2], state[1], lam_of(h))
         return carry
 
+    def take_heads():
+        for off in range(1, nz):
+            zs = (z + off) % nz
+            head_arrival(zs).wait_recv()
+            head_pair(zs).start()
+
+    def step(i, carry):
+        zo = origin(i)
+        take_pair(zo)
+        for f in range(tiles_early):
+            hidden_tile(zo, f)
+
+        take_round(i + 3, 0)
+        take_round(i + 3, 1)
+
+        @pl.when(i + 2 < nz)
+        def _():
+            take_tp(origin(i + 2), 0)
+
+        @pl.when(i > 1)
+        def _():
+            finish(origin(i - 1))
+
+        for f in range(tiles_early, tiles):
+            hidden_tile(zo, f)
+
+        @pl.when(i + 2 < nz)
+        def _():
+            take_tp(origin(i + 2), 1)
+
+        @pl.when(i == 1)
+        def _():
+            finish(z)
+
+        @pl.when(i + 1 < nz)
+        def _():
+            take_pass(origin(i + 1))
+
+        @pl.when(i > 1)
+        def _():
+            middle(origin(i - 2))
+
+        if by_head:
+
+            @pl.when(i == nz - 2)
+            def _():
+                take_heads()
+
+        scale = route_scale(zo)
+        model_tiles(zo, order[:early], scale)
+
+        @pl.when(i > 2)
+        def _():
+            reduce(origin(i - 3))
+
+        model_tiles(zo, order[early:], scale)
+
+        if not by_head:
+            take_kv(zo)
+        return carry
+
+    lax.fori_loop(1, nz, step, 0)
+
+    middle(origin(nz - 2))
+    finish(origin(nz - 1))
     if by_head:
         for n in range(nz):
             head_pair(n, False).wait_recv()
         for n in range(nz):
             position_block(n)
         hrecv[z] = hsend[z]
+        middle(origin(nz - 1))
+        reduce(origin(nz - 3))
         reduce(origin(nz - 2))
-        middle(origin(nz - 1))
         for off in range(1, nz):
             back_arrival((z + off) % nz).wait_recv()
-        head_rows = jnp.concatenate([hrecv[h] for h in range(heads)], axis=1)
+        gathered = hrecv
     else:
 
         def wait_kv(i, carry):
@@ -596,9 +678,11 @@
 
         lax.fori_loop(0, nz, wait_kv, 0)
         lax.fori_loop(0, heads, one_head, 0)
+        reduce(origin(nz - 3))
+        middle(origin(nz - 1))
         reduce(origin(nz - 2))
-        middle(origin(nz - 1))
-        head_rows = jnp.concatenate([hsend[h] for h in range(heads)], axis=1)
+        gathered = hsend
+    head_rows = jnp.concatenate([gathered[h] for h in range(heads)], axis=1)
     weight_copies[3].wait()
     out_rows = tokens // n_tp
 
@@ -616,9 +700,9 @@
         j = (tp + off) % n_tp
         return remote(prod.at[j], abuf.at[j], a_s.at[off], a_r.at[j], ep, j)
 
+    reduce(origin(nz - 1))
     for off in range(1, n_tp):
         row_copy(off).start()
-    reduce(origin(nz - 1))
 
     mixed = prod[tp].astype(F32)
     for off in range(1, n_tp):
@@ -636,7 +720,8 @@
     left = lambda copy: copy.wait_send()
 
     def drain(zo, carry):
-        each_line(x_own, xs_s, xs_r, zo, left)
+        for h in range(2):
+            each_x(zo, h, left)
         each_line(meta, ms_s, ms_r, zo, left)
         for n in range(len(term_parts())):
             term_copy(zo, n).wait_send()
@@ -654,7 +739,8 @@
         def _():
             home_copy(zo).wait_send()
             for n in range(len(targets)):
-                tp_copy(zo, n).wait_send()
+                for h in range(2):
+                    tp_copy(zo, n, h).wait_send()
             if square:
                 for n in range(2):
                     pass_copy(zo, n).wait_send()
@@ -667,6 +753,11 @@
     lax.fori_loop(0, nz, drain, 0)
     for off in range(1, n_tp):
         row_copy(off).wait_send()
+
+
+def settle(rows_ref, exp_ref, out_rows_ref, out_exp_ref):
+    out_rows_ref[...] = rows_ref[...].astype(BF16)
+    out_exp_ref[...] = exp_ref[...].astype(BF16)
 
 
 def body(
@@ -695,11 +786,11 @@
     by_head = heads == nz
     flat = (tokens * heads, width)
     vmem = pl.BlockSpec(memory_space=pltpu.VMEM)
-    smem = pl.BlockSpec(memory_space=pltpu.SMEM)
     hbm = pl.BlockSpec(memory_space=pltpu.HBM)
     dma = pltpu.SemaphoreType.DMA
     line = [dma((2, nz)), dma((nz,))]
     line_sem = [dma((2, nz)), dma((2, nz))]
+    len_targets = 2 if n_tp == 4 else n_tp - 1
     grid_sem = [dma((n_tp, nz)), dma((n_tp, nz))]
     pair = [dma((nz,)), dma((nz,))]
     mixed_rows, mixed_experts = pl.pallas_call(
@@ -708,9 +799,18 @@
             jax.ShapeDtypeStruct((tokens // n_tp, model), F32),
             jax.ShapeDtypeStruct((tokens, quarter), F32),
         ),
-        in_specs=[vmem, vmem, vmem, smem, vmem, vmem, vmem, vmem, vmem, hbm, hbm, hbm, hbm],
+        in_specs=[hbm] * 13,
         out_specs=(vmem, vmem),
         scratch_shapes=[
+            pltpu.VMEM(flat, BF16),
+            pltpu.VMEM(flat, BF16),
+            pltpu.VMEM(flat, BF16),
+            pltpu.VMEM((1, heads), F32),
+            pltpu.VMEM((1, width), F32),
+            pltpu.VMEM((tokens, model), BF16),
+            pltpu.VMEM((1, model), F32),
+            pltpu.VMEM((routes, tokens), jnp.int32),
+            pltpu.VMEM((routes, tokens), F32),
             pltpu.VMEM(out_weight.shape, BF16),
             pltpu.VMEM((model, hidden), BF16),
             pltpu.VMEM((model, hidden), BF16),
@@ -730,21 +830,24 @@
             pltpu.VMEM((nz, tokens, quarter), BF16),
             pltpu.VMEM((n_tp, tokens // n_tp, model), BF16),
             pltpu.VMEM((n_tp, tokens // n_tp, model), BF16),
+            dma((4, nz)),
+            dma((2, nz)),
             *line,
             *line,
-            *line,
-            *grid_sem,
+            dma((2, len_targets, nz)),
+            dma((2, len_targets, nz)),
             *line_sem,
             *grid_sem,
             *pair,
             *pair,
             *grid_sem,
-            dma((max(6, n_tp), nz)),
-            dma((max(6, n_tp), nz)),
+            dma((6 if n_tp == 4 else n_tp, nz)),
+            dma((6 if n_tp == 4 else n_tp, nz)),
             *pair,
             *pair,
             dma((n_tp,)),
             dma((n_tp,)),
+            dma((9,)),
             dma((4,)),
         ],
         compiler_params=pltpu.CompilerParams(
@@ -755,7 +858,7 @@
         query_maps.reshape(flat),
         key_maps.reshape(flat),
         value_rows.reshape(flat),
-        head_lambda,
+        head_lambda.reshape(1, -1),
         head_gain.reshape(1, -1),
         token_rows,
         norm_gain.reshape(1, -1),
@@ -766,7 +869,16 @@
         up_weight[0],
         down_weight[0],
     )
-    return mixed_rows.astype(BF16), mixed_experts.astype(BF16)
+    return pl.pallas_call(
+        settle,
+        out_shape=(
+            jax.ShapeDtypeStruct(mixed_rows.shape, BF16),
+            jax.ShapeDtypeStruct(mixed_experts.shape, BF16),
+        ),
+        in_specs=[vmem, vmem],
+        out_specs=(vmem, vmem),
+        name="settle",
+    )(mixed_rows, mixed_experts)
 
 
 def solution(mesh):

time: 65.5 us -> 60.8 us (0.928)
  other arithmetic: 3.24 us -> 0 us
  Pallas kernels: 61.4 us -> 60 us
    convert_element_type x2 -> x0, other arithmetic: 3.24 us -> none  [body(): return (mixed_rows.astype(BF16), mixed_experts.astype(BF16))]
    pallas_call x1, Pallas kernels: 61.4 us -> 58.3 us  [body(): pl.pallas_call(functools.partial(kernel, n_ep, n_tp, routes, width // 2,...]
    pallas_call x0 -> x1, Pallas kernels: none -> 1.74 us  [body(): pl.pallas_call(settle, out_shape=(jax.ShapeDtypeStruct(mixed_rows.shape,...]
where the time goes in v2:
time: 60.8 us; the launch traced here: 60.7 us
  Pallas kernels  60 us (99%)
  between operations  0.64 us (1%)
    pallas_call x1, Pallas kernels, body(): pl.pallas_call(functools.partial(kernel, n_ep, n_tp, routes, width // 2,...  58.3 us
    pallas_call x1, Pallas kernels, body(): pl.pallas_call(settle, out_shape=(jax.ShapeDtypeStruct(mixed_rows.shape,...  1.74 us

profile of v2, /device:TPU:0, one launch (start us, length us, event | category | flops | bytes accessed | tf_op | source)
XLA Modules:
  0.0 60.7 jit_solution(17579929893773978603)
XLA Ops:
  0.6 58.3 %layer.1 = (f32[32,2048]{1,0:T(8,128)}, f32[128,512]{1,0:T(8,128)}) custom-call(bf16[512,128]{1,0:T(8,128)(2,1)} %bitcast.14, bf16[512,128]{1,0:T(8,128)(2,1)} %bitcast.15, bf16[512,128]{1,0:T(8,128)(2,1)} %bitcast.16, f32[1,4]{1,0:T(1,128)} %bitcast.20, f32[1,128]{1,0:T(1,128)} %bitcast.21, bf16[128,2048]{1,0:T(8,128)(2,1)} %rows_hbm.1, ...), custom_call_target="tpu_custom_call" | custom-call | tf_op jit(solution)/shard_map/layer/pallas_call | solution.py:796
  58.9 1.7 %settle.1 = (bf16[32,2048]{1,0:T(8,128)(2,1)}, bf16[128,512]{1,0:T(8,128)(2,1)}) custom-call(f32[32,2048]{1,0:T(8,128)} %get-tuple-element.4.rows_ref, f32[128,512]{1,0:T(8,128)} %get-tuple-element.5.exp_ref), custom_call_target="tpu_custom_call" | custom-call | tf_op jit(solution)/shard_map/settle/pallas_call | solution.py:872

commit v3 on v2

--- a/solution.py
+++ b/solution.py
@@ -219,13 +219,13 @@
 
     def tp_copy(zo, n, h):
         block = xb.at[tp, zo * CORES + core, halves[h]]
-        return remote(block, block, t_s.at[h, n, zo], t_r.at[h, n, zo], ep, targets[n])
+        return remote(block, block, t_s.at[zo], t_r.at[h, n, zo], ep, targets[n])
 
     def tp_arrival(zo, n, h):
         j = targets[n]
         block = xb.at[j, zo * CORES + core, halves[h]]
         k = n if square else len(targets) - 1 - n
-        return remote(block, block, t_s.at[h, n, zo], t_r.at[h, k, zo], ep, j)
+        return remote(block, block, t_s.at[zo], t_r.at[h, k, zo], ep, j)
 
     def pass_copy(zo, n):
         block = xb.at[other if n == 0 else side, zo * CORES + core, halves[n]]
@@ -237,7 +237,11 @@
 
     def pair_copy(j, zo, mine=True):
         block = xb.at[j, zo * CORES + (core if mine else 1 - core)]
-        return remote(block, block, d_s.at[j, zo], d_r.at[j, zo], partner, tp)
+        return remote(block, block, d_s.at[zo], d_r.at[zo], partner, tp)
+
+    def pair_all(zo, mine=True):
+        block = xb.at[:, zo * CORES + (core if mine else 1 - core)]
+        return remote(block, block, d_s.at[zo], d_r.at[zo], partner, tp)
 
     def pair_block(buf, send, recv, zo, mine=True):
         block = buf.at[zo * CORES + (core if mine else 1 - core)]
@@ -281,8 +285,7 @@
             pair_copy(across, zo).start()
 
     def take_pair(zo):
-        for j in range(n_tp):
-            pair_copy(j, zo, False).wait_recv()
+        pair_all(zo, False).wait_recv()
         pair_block(meta, md_s, md_r, zo, False).wait_recv()
 
     def spread_kv(zo):
@@ -320,7 +323,7 @@
 
     def half_copy(zo, j):
         return remote(
-            cbuf.at[zo, 1 - core, j], pbuf.at[zo, j], p_s.at[j, zo], p_r.at[j, zo], partner, tp
+            cbuf.at[zo, 1 - core, j], pbuf.at[zo, j], p_s.at[zo], p_r.at[j, zo], partner, tp
         )
 
     def term_parts():
@@ -341,7 +344,7 @@
         return remote(
             cbuf.at[zo, core, j, rows_of],
             rbuf.at[zo, slot, rows_of],
-            r_s.at[n, zo],
+            r_s.at[zo],
             r_r.at[n, zo] if square else r_r.at[tp, zo],
             ep,
             device,
@@ -360,7 +363,7 @@
         return remote(
             cbuf.at[zo, core, device, rows_of],
             rbuf.at[zo, slot, rows_of],
-            r_s.at[n, zo],
+            r_s.at[zo],
             sem,
             ep,
             device,
@@ -612,9 +615,7 @@
         def _():
             take_tp(origin(i + 2), 0)
 
-        @pl.when(i > 1)
-        def _():
-            finish(origin(i - 1))
+        finish(origin(i - 1))
 
         for f in range(tiles_early, tiles):
             hidden_tile(zo, f)
@@ -622,10 +623,6 @@
         @pl.when(i + 2 < nz)
         def _():
             take_tp(origin(i + 2), 1)
-
-        @pl.when(i == 1)
-        def _():
-            finish(z)
 
         @pl.when(i + 1 < nz)
         def _():
@@ -664,9 +661,9 @@
         for n in range(nz):
             position_block(n)
         hrecv[z] = hsend[z]
-        middle(origin(nz - 1))
         reduce(origin(nz - 3))
         reduce(origin(nz - 2))
+        middle(origin(nz - 1))
         for off in range(1, nz):
             back_arrival((z + off) % nz).wait_recv()
         gathered = hrecv
@@ -723,11 +720,12 @@
         for h in range(2):
             each_x(zo, h, left)
         each_line(meta, ms_s, ms_r, zo, left)
-        for n in range(len(term_parts())):
-            term_copy(zo, n).wait_send()
-        for j in range(n_tp):
-            pair_copy(j, zo).wait_send()
-            half_copy(zo, j).wait_send()
+        terms = cbuf.at[zo, core, pl.ds(0, n_tp - 1)]
+        remote(terms, terms, r_s.at[zo], r_r.at[0, zo], partner, tp).wait_send()
+        pair_all(zo).wait_send()
+        remote(
+            cbuf.at[zo, 1 - core], pbuf.at[zo], p_s.at[zo], p_r.at[0, zo], partner, tp
+        ).wait_send()
         pair_block(meta, md_s, md_r, zo).wait_send()
         if by_head:
             head_pair(zo).wait_send()
@@ -738,9 +736,8 @@
         @pl.when(zo != z)
         def _():
             home_copy(zo).wait_send()
-            for n in range(len(targets)):
-                for h in range(2):
-                    tp_copy(zo, n, h).wait_send()
+            spread = xb.at[pl.ds(0, len(targets)), zo * CORES + core]
+            remote(spread, spread, t_s.at[zo], t_r.at[0, 0, zo], partner, tp).wait_send()
             if square:
                 for n in range(2):
                     pass_copy(zo, n).wait_send()
@@ -791,7 +788,6 @@
     line = [dma((2, nz)), dma((nz,))]
     line_sem = [dma((2, nz)), dma((2, nz))]
     len_targets = 2 if n_tp == 4 else n_tp - 1
-    grid_sem = [dma((n_tp, nz)), dma((n_tp, nz))]
     pair = [dma((nz,)), dma((nz,))]
     mixed_rows, mixed_experts = pl.pallas_call(
         functools.partial(kernel, n_ep, n_tp, routes, width // 2, by_head),
@@ -834,14 +830,15 @@
             dma((2, nz)),
             *line,
             *line,
-            dma((2, len_targets, nz)),
+            dma((nz,)),
             dma((2, len_targets, nz)),
             *line_sem,
-            *grid_sem,
             *pair,
             *pair,
-            *grid_sem,
-            dma((6 if n_tp == 4 else n_tp, nz)),
+            *pair,
+            dma((nz,)),
+            dma((n_tp, nz)),
+            dma((nz,)),
             dma((6 if n_tp == 4 else n_tp, nz)),
             *pair,
             *pair,

time: 60.8 us -> 58.4 us (0.961)
  Pallas kernels: 60 us -> 57.6 us
    pallas_call x1, Pallas kernels: 58.3 us -> 55.9 us  [body(): pl.pallas_call(functools.partial(kernel, n_ep, n_tp, routes, width // 2,...]
where the time goes in v3:
time: 58.4 us; the launch traced here: 58.3 us
  Pallas kernels  57.6 us (99%)
  between operations  0.64 us (1%)
    pallas_call x1, Pallas kernels, body(): pl.pallas_call(functools.partial(kernel, n_ep, n_tp, routes, width // 2,...  55.9 us
    pallas_call x1, Pallas kernels, body(): pl.pallas_call(settle, out_shape=(jax.ShapeDtypeStruct(mixed_rows.shape,...  1.74 us

profile of v3, /device:TPU:0, one launch (start us, length us, event | category | flops | bytes accessed | tf_op | source)
XLA Modules:
  0.0 58.3 jit_solution(4301905535314739655)
XLA Ops:
  0.6 55.9 %layer.1 = (f32[32,2048]{1,0:T(8,128)}, f32[128,512]{1,0:T(8,128)}) custom-call(bf16[512,128]{1,0:T(8,128)(2,1)} %bitcast.14, bf16[512,128]{1,0:T(8,128)(2,1)} %bitcast.15, bf16[512,128]{1,0:T(8,128)(2,1)} %bitcast.16, f32[1,4]{1,0:T(1,128)} %bitcast.20, f32[1,128]{1,0:T(1,128)} %bitcast.21, bf16[128,2048]{1,0:T(8,128)(2,1)} %rows_hbm.1, ...), custom_call_target="tpu_custom_call" | custom-call | tf_op jit(solution)/shard_map/layer/pallas_call | solution.py:792
  56.5 1.7 %settle.1 = (bf16[32,2048]{1,0:T(8,128)(2,1)}, bf16[128,512]{1,0:T(8,128)(2,1)}) custom-call(f32[32,2048]{1,0:T(8,128)} %get-tuple-element.4.rows_ref, f32[128,512]{1,0:T(8,128)} %get-tuple-element.5.exp_ref), custom_call_target="tpu_custom_call" | custom-call | tf_op jit(solution)/shard_map/settle/pallas_call | solution.py:869
